TPU v7x, 32 devices: a whole 2x2x4 slice. The times are simulated.
32 devices in a mesh: fs: 8 (over z, x), tp: 4 (over y, core).
Axes of the slice: x: 2, y: 2, z: 4, core: 2. Of those that a mesh axis runs over, the one named last changes fastest.
Arguments:
- prompt_rows: bfloat16 [512, 3072], P('tp'), may hold values from -6 to 6
- gate_first: float32 [3072, 8192], P('fs', 'tp'), may hold values from -0.109375 to 0.109375
- up_first: float32 [3072, 8192], P('fs', 'tp'), may hold values from -0.109375 to 0.109375
- down_first: float32 [8192, 3072], P('fs', 'tp'), may hold values from -0.0625 to 0.0625
- gate_second: float32 [3072, 8192], P('fs', 'tp'), may hold values from -0.109375 to 0.109375
- up_second: float32 [3072, 8192], P('fs', 'tp'), may hold values from -0.109375 to 0.109375
- down_second: float32 [8192, 3072], P('fs', 'tp'), may hold values from -0.0625 to 0.0625
- pre_gain_first: float32 [3072], replicated, may hold values from 0.1 to 1.9
- post_gain_first: float32 [3072], replicated, may hold values from 0.1 to 1.9
- pre_gain_second: float32 [3072], replicated, may hold values from 0.1 to 1.9
- post_gain_second: float32 [3072], replicated, may hold values from 0.1 to 1.9
Outputs:
- result_rows: bfloat16 [512, 3072], P('tp')
- gate_first_new: bfloat16 [3072, 8192], P(None, 'fs')
- up_first_new: bfloat16 [3072, 8192], P(None, 'fs')
- down_first_new: bfloat16 [8192, 3072], P('fs')
- gate_second_new: bfloat16 [3072, 8192], P(None, 'fs')
- up_second_new: bfloat16 [3072, 8192], P(None, 'fs')
- down_second_new: bfloat16 [8192, 3072], P('fs')
All inputs are finite; a program needn't handle non-finite values.
Results may differ from a plain program's by a relative error of at most 0.0071.
Values may be sent and summed in bfloat16 or wider, within the bound.
A program may use at most 192 MiB of HBM per device.

v0:
```python
import jax
import jax.numpy as jnp
from jax import lax
from jax.sharding import PartitionSpec as P

EPSILON = 1e-06


def half_step(rows, gate, up, down, post_gain):
    floats = rows.astype(jnp.float32)
    normed = (
        floats * lax.rsqrt(jnp.mean(floats * floats, axis=-1, keepdims=True) + EPSILON)
    ).astype(jnp.bfloat16)
    gate_pre = jnp.dot(normed, gate, preferred_element_type=jnp.float32)
    up_pre = jnp.dot(normed, up, preferred_element_type=jnp.float32)
    hidden = (jax.nn.silu(gate_pre) * up_pre).astype(jnp.bfloat16)
    partial_value = jnp.dot(hidden, down, preferred_element_type=jnp.float32)
    total = lax.psum(partial_value, "fs")
    scale = lax.rsqrt(jnp.mean(total * total, axis=-1, keepdims=True) + EPSILON)
    return (floats + 0.5 * total * scale * post_gain[None, :]).astype(jnp.bfloat16)


def per_device(
    prompt_rows,
    gate_first,
    up_first,
    down_first,
    gate_second,
    up_second,
    down_second,
    pre_gain_first,
    post_gain_first,
    pre_gain_second,
    post_gain_second,
):
    height = gate_first.shape[0]
    start = lax.axis_index("fs") * height
    gain_a = lax.dynamic_slice_in_dim(pre_gain_first, start, height, 0)[:, None]
    gain_b = lax.dynamic_slice_in_dim(pre_gain_second, start, height, 0)[:, None]
    wide = (
        lax.all_gather((gain_a * gate_first).astype(jnp.bfloat16), "tp", axis=1, tiled=True),
        lax.all_gather((gain_a * up_first).astype(jnp.bfloat16), "tp", axis=1, tiled=True),
        lax.all_gather(down_first.astype(jnp.bfloat16), "tp", axis=1, tiled=True),
        lax.all_gather((gain_b * gate_second).astype(jnp.bfloat16), "tp", axis=1, tiled=True),
        lax.all_gather((gain_b * up_second).astype(jnp.bfloat16), "tp", axis=1, tiled=True),
        lax.all_gather(down_second.astype(jnp.bfloat16), "tp", axis=1, tiled=True),
    )
    gate_a, up_a, gate_b, up_b = (
        lax.all_to_all(wide[0], "fs", split_axis=1, concat_axis=0, tiled=True),
        lax.all_to_all(wide[1], "fs", split_axis=1, concat_axis=0, tiled=True),
        lax.all_to_all(wide[3], "fs", split_axis=1, concat_axis=0, tiled=True),
        lax.all_to_all(wide[4], "fs", split_axis=1, concat_axis=0, tiled=True),
    )
    down_a = wide[2]
    down_b = wide[5]
    middle = half_step(prompt_rows, gate_a, up_a, down_a, post_gain_first)
    result = half_step(middle, gate_b, up_b, down_b, post_gain_second)
    return (result, gate_a, up_a, down_a, gate_b, up_b, down_b)


def solution(mesh):
    return jax.shard_map(
        per_device,
        mesh=mesh,
        in_specs=(
            P("tp", None),
            P("fs", "tp"),
            P("fs", "tp"),
            P("fs", "tp"),
            P("fs", "tp"),
            P("fs", "tp"),
            P("fs", "tp"),
            P(),
            P(),
            P(),
            P(),
        ),
        out_specs=(
            P("tp", None),
            P(None, "fs"),
            P(None, "fs"),
            P("fs", None),
            P(None, "fs"),
            P(None, "fs"),
            P("fs", None),
        ),
        check_vma=False,
    )
```

profile of v0, /device:TPU:0, one launch (start us, length us, event | category | flops | bytes accessed | tf_op | source)
XLA Modules:
  0.0 843.3 jit_solution(3647729259422297711)
XLA Ops:
  8.0 5.5 multiply_convert_fusion.3
  14.3 48.5 %all-gather.7.cloned.1.call-done = bf16[384,8192]{1,0:T(8,128)(2,1)} async-done(((bf16[384,2048]{1,0:T(8,128)(2,1)}), bf16[384,8192]{1,0:T(8,128)(2,1)}) %all-gather.7.cloned.1.call-update) | async-done | bytes 6291472 | tf_op jit(solution)/shard_map/all_gather | solution.py:41
  62.7 6.5 copy.33
  69.2 5.8 all-to-all-start
  80.4 30.9 %all-gather.9.cloned.1.call-done = bf16[384,8192]{1,0:T(8,128)(2,1)} async-done(((bf16[384,2048]{1,0:T(8,128)(2,1)}), bf16[384,8192]{1,0:T(8,128)(2,1)}) %all-gather.9.cloned.1.call-update) | async-done | bytes 6291472 | tf_op jit(solution)/shard_map/all_gather | solution.py:42
  111.3 6.5 copy.32
  117.8 95.9 %all-to-all-done = bf16[384,8,1024]{2,0,1:T(8,128)(2,1)} async-done(((bf16[384,8,1024]{2,0,1:T(8,128)(2,1)}), bf16[384,8,1024]{2,0,1:T(8,128)(2,1)}, u32[]{:S(2)}, u32[]{:S(2)}) %all-to-all-start) | async-done | bytes 6291488 | tf_op jit(solution)/shard_map/all_to_all | solution.py:49
  213.7 4.8 all-to-all-start.1
  219.0 6.5 copy.31
  225.5 130.6 %all-to-all-done.1 = bf16[384,8,1024]{2,0,1:T(8,128)(2,1)} async-done(((bf16[384,8,1024]{2,0,1:T(8,128)(2,1)}), bf16[384,8,1024]{2,0,1:T(8,128)(2,1)}, u32[]{:S(2)}, u32[]{:S(2)}) %all-to-all-start.1) | async-done | bytes 6291488 | tf_op jit(solution)/shard_map/all_to_all | solution.py:50
  356.1 4.8 all-to-all-start.2
  364.6 6.5 copy.30
  375.7 35.5 %all-gather.11.cloned.1.call-done = bf16[1024,3072]{1,0:T(8,128)(2,1)} async-done(((bf16[1024,768]{1,0:T(8,128)(2,1)}), bf16[1024,3072]{1,0:T(8,128)(2,1)}) %all-gather.11.cloned.1.call-update) | async-done | bytes 6291472 | tf_op jit(solution)/shard_map/all_gather | solution.py:43
  411.2 7.7 fusion.9
  418.9 100.4 %all-to-all-done.2 = bf16[384,8,1024]{2,0,1:T(8,128)(2,1)} async-done(((bf16[384,8,1024]{2,0,1:T(8,128)(2,1)}), bf16[384,8,1024]{2,0,1:T(8,128)(2,1)}, u32[]{:S(2)}, u32[]{:S(2)}) %all-to-all-start.2) | async-done | bytes 6291488 | tf_op jit(solution)/shard_map/all_to_all | solution.py:51
  519.3 4.8 all-to-all-start.3
  527.7 130.8 %all-reduce.3.cloned.1.call-done = f32[128,3072]{1,0:T(8,128)} async-done(((f32[128,3072]{1,0:T(8,128)}), f32[128,3072]{1,0:T(8,128)}) %all-reduce.3.cloned.1.call-update) | async-done | bytes 1572880 | tf_op jit(solution)/shard_map/psum | solution.py:18
  666.3 38.0 %all-gather.17.cloned.1.call-done = bf16[1024,3072]{1,0:T(8,128)(2,1)} async-done(((bf16[1024,768]{1,0:T(8,128)(2,1)}), bf16[1024,3072]{1,0:T(8,128)(2,1)}) %all-gather.17.cloned.1.call-update) | async-done | bytes 6291472 | tf_op jit(solution)/shard_map/all_gather | solution.py:46
  704.2 7.7 fusion.8
  712.0 89.4 %all-reduce.5.cloned.1.call-done = f32[128,3072]{1,0:T(8,128)} async-done(((f32[128,3072]{1,0:T(8,128)}), f32[128,3072]{1,0:T(8,128)}) %all-reduce.5.cloned.1.call-update) | async-done | bytes 1572880 | tf_op jit(solution)/shard_map/psum | solution.py:18
  805.6 6.4 copy.42
  812.0 6.3 copy.43
  821.0 6.4 copy.45
  827.4 6.3 copy.46
  (55 shorter events, 36.7 us)
Async XLA Ops:
  7.2 55.6 %all-gather.7.cloned.1.call-start = ((), (), s32[]{:S(2)}) async-start(), calls=%async_computation.4 | async-start | bytes 7864320 | tf_op jit(solution)/shard_map/all_gather | solution.py:41
  13.5 97.8 %all-gather.9.cloned.1.call-start = ((), (), s32[]{:S(2)}) async-start(), calls=%async_computation.5 | async-start | bytes 7864320 | tf_op jit(solution)/shard_map/all_gather | solution.py:42
  69.2 6.6 copy-start.1
  69.2 144.4 %all-to-all-start = ((bf16[384,8,1024]{2,0,1:T(8,128)(2,1)}), bf16[384,8,1024]{2,0,1:T(8,128)(2,1)}, u32[]{:S(2)}, u32[]{:S(2)}) async-start(bf16[384,8,1024]{2,0,1:T(8,128)(2,1)} %bitcast.40), calls=%async_computation | async-start | bytes 12582912 | tf_op jit(solution)/shard_map/all_to_all | solution.py:49
  75.0 144.0 %all-gather.13.cloned.1.call-start = ((), (), s32[]{:S(2)}) async-start(), calls=%async_computation.8 | async-start | bytes 7864320 | tf_op jit(solution)/shard_map/all_gather | solution.py:44
  213.7 142.5 %all-to-all-start.1 = ((bf16[384,8,1024]{2,0,1:T(8,128)(2,1)}), bf16[384,8,1024]{2,0,1:T(8,128)(2,1)}, u32[]{:S(2)}, u32[]{:S(2)}) async-start(bf16[384,8,1024]{2,0,1:T(8,128)(2,1)} %bitcast.41), calls=%async_computation.1 | async-start | bytes 12582912 | tf_op jit(solution)/shard_map/all_to_all | solution.py:50
  218.4 146.2 %all-gather.15.cloned.1.call-start = ((), (), s32[]{:S(2)}) async-start(), calls=%async_computation.9 | async-start | bytes 7864320 | tf_op jit(solution)/shard_map/all_gather | solution.py:45
  356.1 163.1 %all-to-all-start.2 = ((bf16[384,8,1024]{2,0,1:T(8,128)(2,1)}), bf16[384,8,1024]{2,0,1:T(8,128)(2,1)}, u32[]{:S(2)}, u32[]{:S(2)}) async-start(bf16[384,8,1024]{2,0,1:T(8,128)(2,1)} %bitcast.39), calls=%async_computation.2 | async-start | bytes 12582912 | tf_op jit(solution)/shard_map/all_to_all | solution.py:51
  361.0 3.4 copy-start
  361.0 50.2 %all-gather.11.cloned.1.call-start = ((), (), s32[]{:S(2)}) async-start(), calls=%async_computation.6 | async-start | bytes 7864320 | tf_op jit(solution)/shard_map/all_gather | solution.py:43
  364.3 294.2 %all-reduce.3.cloned.1.call-start = ((), (), s32[]{:S(2)}) async-start(), calls=%async_computation.7 | async-start | bytes 3145728 | tf_op jit(solution)/shard_map/psum | solution.py:18
  519.3 185.0 %all-to-all-start.3 = ((bf16[384,8,1024]{2,0,1:T(8,128)(2,1)}), bf16[384,8,1024]{2,0,1:T(8,128)(2,1)}, u32[]{:S(2)}, u32[]{:S(2)}) async-start(bf16[384,8,1024]{2,0,1:T(8,128)(2,1)} %bitcast.38), calls=%async_computation.3 | async-start | bytes 12582912 | tf_op jit(solution)/shard_map/all_to_all | solution.py:52
  524.1 136.0 %copy-start.2 = (f32[3072]{0:T(1024)S(1)}, f32[3072]{0:T(1024)}, u32[]{:S(2)}) copy-start(f32[3072]{0:T(1024)} %param.19) | copy-start | bytes 36868
  524.1 180.1 %all-gather.17.cloned.1.call-start = ((), (), s32[]{:S(2)}) async-start(), calls=%async_computation.10 | async-start | bytes 7864320 | tf_op jit(solution)/shard_map/all_gather | solution.py:46
  527.4 273.9 %all-reduce.5.cloned.1.call-start = ((), (), s32[]{:S(2)}) async-start(), calls=%async_computation.11 | async-start | bytes 3145728 | tf_op jit(solution)/shard_map/psum | solution.py:18
  711.9 91.1 %copy-start.3 = (f32[3072]{0:T(1024)S(1)}, f32[3072]{0:T(1024)}, u32[]{:S(2)}) copy-start(f32[3072]{0:T(1024)} %param.21) | copy-start | bytes 36868
  805.6 12.7 %slice-start = ((s8[6291456]{0:T(1024)(128)(4,1)}), s8[4194304]{0:T(1024)(128)(4,1)S(1)}, s32[]{:S(2)}) async-start(s8[6291456]{0:T(1024)(128)(4,1)} %bitcast.34), calls=%async_computation.12 | async-start | bytes 8388608
  812.0 6.4 slice-start.1
  821.0 12.7 %slice-start.2 = ((s8[6291456]{0:T(1024)(128)(4,1)}), s8[4194304]{0:T(1024)(128)(4,1)S(1)}, s32[]{:S(2)}) async-start(s8[6291456]{0:T(1024)(128)(4,1)} %bitcast.36), calls=%async_computation.14 | async-start | bytes 8388608
  827.4 6.4 slice-start.3
Sparse Core Ops, SparseCore 0:
  13.6 49.0 all-gather.6
  64.9 46.3 all-gather.8
  113.4 46.3 all-gather.12
  221.1 46.7 all-gather.14
  364.4 46.6 all-gather.10
  419.0 239.4 all-reduce.2
  660.6 43.5 all-gather.16
  712.1 89.2 all-reduce.4
where the time goes:
time: 844 us; the launch traced here: 843 us
  waiting for transfers between devices  701 us (83%)
  local copies, waits for them, and re-layouts  58.5 us (7%)
  other arithmetic  24.5 us (3%)
  matrix products  24.2 us (3%)
  starting transfers between devices  20.7 us (2%)
  between operations  14.3 us (2%)
    psum x2, waiting for transfers between devices, half_step(): total = lax.psum(partial_value, 'fs')  220 us
    all_to_all x1, waiting for transfers between devices, per_device(): lax.all_to_all(wide[1], 'fs', split_axis=1, concat_axis=0, tiled=True)  131 us
    all_to_all x1, waiting for transfers between devices, per_device(): lax.all_to_all(wide[3], 'fs', split_axis=1, concat_axis=0, tiled=True)  100 us
    all_to_all x1, waiting for transfers between devices, per_device(): lax.all_to_all(wide[0], 'fs', split_axis=1, concat_axis=0, tiled=True)  95.9 us
    all_gather x1, waiting for transfers between devices, per_device(): lax.all_gather((gain_a * gate_first).astype(jnp.bfloat16), 'tp', axis=1,...  48.5 us
    all_gather x1, waiting for transfers between devices, per_device(): lax.all_gather(down_second.astype(jnp.bfloat16), 'tp', axis=1, tiled=True)  38 us
    all_gather x1, waiting for transfers between devices, per_device(): lax.all_gather(down_first.astype(jnp.bfloat16), 'tp', axis=1, tiled=True)  35.5 us
    unnamed x22, local copies, waits for them, and re-layouts  30.9 us
  transfers between devices with their start and end apart: 12, of which 9 were waited for; matrix products, arithmetic and copies ran while one was open for 7% of the time, Pallas kernels for 0%

commit v1 on v0

--- a/solution.py
+++ b/solution.py
@@ -15,7 +15,7 @@
     up_pre = jnp.dot(normed, up, preferred_element_type=jnp.float32)
     hidden = (jax.nn.silu(gate_pre) * up_pre).astype(jnp.bfloat16)
     partial_value = jnp.dot(hidden, down, preferred_element_type=jnp.float32)
-    total = lax.psum(partial_value, "fs")
+    total = jnp.sum(lax.all_gather(partial_value, "fs"), axis=0)
     scale = lax.rsqrt(jnp.mean(total * total, axis=-1, keepdims=True) + EPSILON)
     return (floats + 0.5 * total * scale * post_gain[None, :]).astype(jnp.bfloat16)
 

time: 844 us -> 1030 us (1.22)
  waiting for transfers between devices: 701 us -> 878 us
    psum x2 -> x0, waiting for transfers between devices: 220 us -> none  [half_step(): total = lax.psum(partial_value, 'fs')]
    all_gather x0 -> x2, waiting for transfers between devices: none -> 208 us  [half_step(): total = jnp.sum(lax.all_gather(partial_value, 'fs'), axis=0)]
    all_to_all x1, waiting for transfers between devices: 100 us -> 264 us  [per_device(): lax.all_to_all(wide[3], 'fs', split_axis=1, concat_axis=0, tiled=True)]
    all_gather x1, waiting for transfers between devices: 35.5 us -> 0.02 us  [per_device(): lax.all_gather(down_first.astype(jnp.bfloat16), 'tp', axis=1, tiled=True)]
    all_gather x1, waiting for transfers between devices: 38 us -> 69.8 us  [per_device(): lax.all_gather(down_second.astype(jnp.bfloat16), 'tp', axis=1, tiled=True)]
    all_to_all x1, waiting for transfers between devices: 0.01 us -> 29.5 us  [per_device(): lax.all_to_all(wide[4], 'fs', split_axis=1, concat_axis=0, tiled=True)]
    reduce_sum x0 -> x2, other arithmetic: none -> 11.9 us  [half_step(): total = jnp.sum(lax.all_gather(partial_value, 'fs'), axis=0)]
    unnamed x22 -> x24, local copies, waits for them, and re-layouts: 30.9 us -> 31.9 us
  transfers between devices with their start and end apart: 12 -> 12, of which waited for: 9 -> 9; matrix products, arithmetic and copies ran while one was open for 7% -> 6% of each run, Pallas kernels for 0% -> 0%
where the time goes in v1:
time: 1030 us
  waiting for transfers between devices  878 us (85%)
  local copies, waits for them, and re-layouts  59.8 us (6%)
  other arithmetic  28.8 us (3%)
  matrix products  23.1 us (2%)
  starting transfers between devices  20.9 us (2%)
  between operations  14.2 us (1%)
    all_to_all x1, waiting for transfers between devices, per_device(): lax.all_to_all(wide[3], 'fs', split_axis=1, concat_axis=0, tiled=True)  264 us
    all_gather x2, waiting for transfers between devices, half_step(): total = jnp.sum(lax.all_gather(partial_value, 'fs'), axis=0)  208 us
    all_to_all x1, waiting for transfers between devices, per_device(): lax.all_to_all(wide[1], 'fs', split_axis=1, concat_axis=0, tiled=True)  133 us
    all_to_all x1, waiting for transfers between devices, per_device(): lax.all_to_all(wide[0], 'fs', split_axis=1, concat_axis=0, tiled=True)  95.9 us
    all_gather x1, waiting for transfers between devices, per_device(): lax.all_gather(down_second.astype(jnp.bfloat16), 'tp', axis=1, tiled=True)  69.8 us
    all_gather x1, waiting for transfers between devices, per_device(): lax.all_gather((gain_a * gate_first).astype(jnp.bfloat16), 'tp', axis=1,...  46 us
    unnamed x24, local copies, waits for them, and re-layouts  31.9 us
    all_gather x1, waiting for transfers between devices, per_device(): lax.all_gather((gain_a * up_first).astype(jnp.bfloat16), 'tp', axis=1, ti...  30.9 us
  transfers between devices with their start and end apart: 12, of which 9 were waited for; matrix products, arithmetic and copies ran while one was open for 6% of the time, Pallas kernels for 0%

profile of v1, /device:TPU:0, one launch (start us, length us, event | category | flops | bytes accessed | tf_op | source)
XLA Modules:
  0.0 1025.1 jit_solution(3632938610966043488)
XLA Ops:
  8.0 5.5 multiply_convert_fusion.3
  16.7 46.0 %all-gather.11.cloned.1.call-done = bf16[384,8192]{1,0:T(8,128)(2,1)} async-done(((bf16[384,2048]{1,0:T(8,128)(2,1)}), bf16[384,8192]{1,0:T(8,128)(2,1)}) %all-gather.11.cloned.1.call-update) | async-done | bytes 6291472 | tf_op jit(solution)/shard_map/all_gather | solution.py:41
  62.7 6.5 copy.33
  69.2 5.8 all-to-all-start
  80.4 30.9 %all-gather.13.cloned.1.call-done = bf16[384,8192]{1,0:T(8,128)(2,1)} async-done(((bf16[384,2048]{1,0:T(8,128)(2,1)}), bf16[384,8192]{1,0:T(8,128)(2,1)}) %all-gather.13.cloned.1.call-update) | async-done | bytes 6291472 | tf_op jit(solution)/shard_map/all_gather | solution.py:42
  111.3 6.5 copy.32
  117.8 95.9 %all-to-all-done = bf16[384,8,1024]{2,0,1:T(8,128)(2,1)} async-done(((bf16[384,8,1024]{2,0,1:T(8,128)(2,1)}), bf16[384,8,1024]{2,0,1:T(8,128)(2,1)}, u32[]{:S(2)}, u32[]{:S(2)}) %all-to-all-start) | async-done | bytes 6291488 | tf_op jit(solution)/shard_map/all_to_all | solution.py:49
  213.7 5.0 all-to-all-start.1
  223.4 133.0 %all-to-all-done.1 = bf16[384,8,1024]{2,0,1:T(8,128)(2,1)} async-done(((bf16[384,8,1024]{2,0,1:T(8,128)(2,1)}), bf16[384,8,1024]{2,0,1:T(8,128)(2,1)}, u32[]{:S(2)}, u32[]{:S(2)}) %all-to-all-start.1) | async-done | bytes 6291488 | tf_op jit(solution)/shard_map/all_to_all | solution.py:50
  356.3 7.7 fusion.9
  364.1 6.7 copy.31
  375.8 6.5 copy.30
  382.3 263.5 %all-to-all-done.2 = bf16[384,8,1024]{2,0,1:T(8,128)(2,1)} async-done(((bf16[384,8,1024]{2,0,1:T(8,128)(2,1)}), bf16[384,8,1024]{2,0,1:T(8,128)(2,1)}, u32[]{:S(2)}, u32[]{:S(2)}) %all-to-all-start.2) | async-done | bytes 6291488 | tf_op jit(solution)/shard_map/all_to_all | solution.py:51
  654.1 33.6 %all-gather.23.cloned.1.call-done = f32[1024,3072]{1,0:T(8,128)} async-done(((f32[128,3072]{1,0:T(8,128)}), f32[1024,3072]{1,0:T(8,128)}) %all-gather.23.cloned.1.call-update) | async-done | bytes 12582928 | tf_op jit(solution)/shard_map/all_gather | solution.py:18
  687.7 6.0 reduce_sum.55
  698.2 69.8 %all-gather.21.cloned.1.call-done = bf16[1024,3072]{1,0:T(8,128)(2,1)} async-done(((bf16[1024,768]{1,0:T(8,128)(2,1)}), bf16[1024,3072]{1,0:T(8,128)(2,1)}) %all-gather.21.cloned.1.call-update) | async-done | bytes 6291472 | tf_op jit(solution)/shard_map/all_gather | solution.py:46
  768.1 29.5 %all-to-all-done.3 = bf16[384,8,1024]{2,0,1:T(8,128)(2,1)} async-done(((bf16[384,8,1024]{2,0,1:T(8,128)(2,1)}), bf16[384,8,1024]{2,0,1:T(8,128)(2,1)}, u32[]{:S(2)}, u32[]{:S(2)}) %all-to-all-start.3) | async-done | bytes 6291488 | tf_op jit(solution)/shard_map/all_to_all | solution.py:52
  797.6 7.7 fusion.8
  805.3 174.7 %all-gather.25.cloned.1.call-done = f32[1024,3072]{1,0:T(8,128)} async-done(((f32[128,3072]{1,0:T(8,128)}), f32[1024,3072]{1,0:T(8,128)}) %all-gather.25.cloned.1.call-update) | async-done | bytes 12582928 | tf_op jit(solution)/shard_map/all_gather | solution.py:18
  980.0 6.0 reduce_sum.58
  987.4 6.4 copy.40
  993.8 6.3 copy.41
  1002.8 6.4 copy.43
  1009.2 6.3 copy.44
  (59 shorter events, 38.6 us)
Async XLA Ops:
  7.2 55.6 %all-gather.11.cloned.1.call-start = ((), (), s32[]{:S(2)}) async-start(), calls=%async_computation.4 | async-start | bytes 7864320 | tf_op jit(solution)/shard_map/all_gather | solution.py:41
  13.5 1.9 copy-start.2
  13.5 97.8 %all-gather.13.cloned.1.call-start = ((), (), s32[]{:S(2)}) async-start(), calls=%async_computation.5 | async-start | bytes 7864320 | tf_op jit(solution)/shard_map/all_gather | solution.py:42
  14.3 209.1 %all-gather.15.cloned.1.call-start = ((), (), s32[]{:S(2)}) async-start(), calls=%async_computation.6 | async-start | bytes 7864320 | tf_op jit(solution)/shard_map/all_gather | solution.py:43
  69.2 6.6 copy-start.1
  69.2 144.4 %all-to-all-start = ((bf16[384,8,1024]{2,0,1:T(8,128)(2,1)}), bf16[384,8,1024]{2,0,1:T(8,128)(2,1)}, u32[]{:S(2)}, u32[]{:S(2)}) async-start(bf16[384,8,1024]{2,0,1:T(8,128)(2,1)} %bitcast.42), calls=%async_computation | async-start | bytes 12582912 | tf_op jit(solution)/shard_map/all_to_all | solution.py:49
  75.0 289.1 %all-gather.17.cloned.1.call-start = ((), (), s32[]{:S(2)}) async-start(), calls=%async_computation.7 | async-start | bytes 7864320 | tf_op jit(solution)/shard_map/all_gather | solution.py:44
  213.7 5.6 copy-start
  213.7 142.7 %all-to-all-start.1 = ((bf16[384,8,1024]{2,0,1:T(8,128)(2,1)}), bf16[384,8,1024]{2,0,1:T(8,128)(2,1)}, u32[]{:S(2)}, u32[]{:S(2)}) async-start(bf16[384,8,1024]{2,0,1:T(8,128)(2,1)} %bitcast.41), calls=%async_computation.1 | async-start | bytes 12582912 | tf_op jit(solution)/shard_map/all_to_all | solution.py:50
  218.6 157.2 %all-gather.19.cloned.1.call-start = ((), (), s32[]{:S(2)}) async-start(), calls=%async_computation.8 | async-start | bytes 7864320 | tf_op jit(solution)/shard_map/all_gather | solution.py:45
  219.2 468.5 %all-gather.23.cloned.1.call-start = ((), (), s32[]{:S(2)}) async-start(), calls=%async_computation.10 | async-start | bytes 14155776 | tf_op jit(solution)/shard_map/all_gather | solution.py:18
  370.9 275.0 %all-to-all-start.2 = ((bf16[384,8,1024]{2,0,1:T(8,128)(2,1)}), bf16[384,8,1024]{2,0,1:T(8,128)(2,1)}, u32[]{:S(2)}, u32[]{:S(2)}) async-start(bf16[384,8,1024]{2,0,1:T(8,128)(2,1)} %bitcast.43), calls=%async_computation.2 | async-start | bytes 12582912 | tf_op jit(solution)/shard_map/all_to_all | solution.py:51
  645.9 151.7 %all-to-all-start.3 = ((bf16[384,8,1024]{2,0,1:T(8,128)(2,1)}), bf16[384,8,1024]{2,0,1:T(8,128)(2,1)}, u32[]{:S(2)}, u32[]{:S(2)}) async-start(bf16[384,8,1024]{2,0,1:T(8,128)(2,1)} %bitcast.40), calls=%async_computation.3 | async-start | bytes 12582912 | tf_op jit(solution)/shard_map/all_to_all | solution.py:52
  650.6 117.4 %all-gather.21.cloned.1.call-start = ((), (), s32[]{:S(2)}) async-start(), calls=%async_computation.9 | async-start | bytes 7864320 | tf_op jit(solution)/shard_map/all_gather | solution.py:46
  653.9 326.1 %all-gather.25.cloned.1.call-start = ((), (), s32[]{:S(2)}) async-start(), calls=%async_computation.11 | async-start | bytes 14155776 | tf_op jit(solution)/shard_map/all_gather | solution.py:18
  687.7 6.2 copy-start.3
  980.0 6.2 copy-start.4
  987.4 12.7 %slice-start = ((s8[6291456]{0:T(1024)(128)(4,1)}), s8[4194304]{0:T(1024)(128)(4,1)S(1)}, s32[]{:S(2)}) async-start(s8[6291456]{0:T(1024)(128)(4,1)} %bitcast.36), calls=%async_computation.12 | async-start | bytes 8388608
  993.8 6.4 slice-start.1
  1002.8 12.7 %slice-start.2 = ((s8[6291456]{0:T(1024)(128)(4,1)}), s8[4194304]{0:T(1024)(128)(4,1)S(1)}, s32[]{:S(2)}) async-start(s8[6291456]{0:T(1024)(128)(4,1)} %bitcast.38), calls=%async_computation.14 | async-start | bytes 8388608
  1009.2 6.4 slice-start.3
Sparse Core Ops, SparseCore 0:
  13.6 49.0 all-gather.10
  64.9 46.3 all-gather.12
  113.4 46.3 all-gather.14
  161.8 46.3 all-gather.16
  221.3 46.7 all-gather.18
  364.2 323.4 all-gather.22
  689.9 78.1 all-gather.20
  805.4 174.5 all-gather.24
